TPU v7x, 32 devices: a whole 2x2x4 slice. The times are simulated.
32 devices in a mesh: ep: 16 (over z, y, x), tp: 2 (over core).
Axes of the slice: x: 2, y: 2, z: 4, core: 2. Of those that a mesh axis runs over, the one named last changes fastest.
Arguments:
- tokens: bfloat16 [512, 2048], P('ep'), may hold values from -6 to 6
- lengths: int32 [512], P('ep'), may hold values from 128 to 1024
- key_cache: bfloat16 [512, 1024, 256], P('ep', None, 'tp'), may hold values from -1000 to 1000
- value_cache: bfloat16 [512, 1024, 256], P('ep', None, 'tp'), may hold values from -6 to 6
- gate_cache: float32 [512, 16, 1024], P('ep', 'tp'), may hold values from -130 to 0, as said below
- mix_gain: float32 [2048], replicated, may hold values from 0.1 to 1.9
- query_weight: bfloat16 [2048, 1024], P(None, 'tp'), may hold values from -0.125 to 0.125
- key_weight: bfloat16 [2048, 256], P(None, 'tp'), may hold values from -0.125 to 0.125
- value_weight: bfloat16 [2048, 256], P(None, 'tp'), may hold values from -0.125 to 0.125
- forget_weight: bfloat16 [2048, 16], P(None, 'tp'), may hold values from -0.125 to 0.125
- out_weight: bfloat16 [1024, 2048], P('tp'), may hold values from -0.1875 to 0.1875
- expert_gain: float32 [2048], replicated, may hold values from 0.1 to 1.9
- routes: int32 [512, 2], P('ep'), may hold values from 0 to 7, all different within a row; in each aligned block of 32 rows (0 to 31, 32 to 63, ...) at most 12 rows name the same one
- route_weights: float32 [512, 2], P('ep'), may hold values from 0.2 to 1
- expert_gate: bfloat16 [2048, 65536], P(None, ('ep', 'tp')), may hold values from -0.125 to 0.125
- expert_up: bfloat16 [2048, 65536], P(None, ('ep', 'tp')), may hold values from -0.125 to 0.125
- expert_down: bfloat16 [65536, 2048], P(('ep', 'tp')), may hold values from -0.0625 to 0.0625
Outputs:
- layer_out: bfloat16 [512, 2048], P('ep')
Inputs may be any that keep to these rules, and one draw needn't show every extreme that they name: `routes`: within the rows of one index of ep, no expert is named more than 12 times, and in every draw some expert is named exactly 12 times in some such rows; the 2 experts of a row differ. `gate_cache`: for each sequence and head the values never rise along the cache positions.
All inputs are finite; a program needn't handle non-finite values.
Results may differ from a plain program's by a relative error of at most 0.013.
Values may be sent and summed in bfloat16 or wider, within the bound.
A program may use at most 128 MiB of HBM per device.

v0:
```python
import jax
import jax.numpy as jnp
from jax import lax
from jax.sharding import PartitionSpec as P

HD = 64
EXPERTS = 8
CAP = 12
eps = 1e-06


def normed(values, gain):
    floats = values.astype(jnp.float32)
    return floats * lax.rsqrt(jnp.mean(floats * floats, axis=-1, keepdims=True) + eps) * gain


def attend(queries, key_new, value_new, log_gate, key_rows, value_rows, cumulative, length):
    seq_count, head_count, head_size = queries.shape
    kv_count = key_new.shape[1]
    group_size = head_count // kv_count
    cache_locations = key_rows.shape[1]
    factor = head_size ** (-0.5)
    grouped = queries.reshape(seq_count, kv_count, group_size, head_size)
    key_split = key_rows.reshape(seq_count, cache_locations, kv_count, head_size)
    value_split = value_rows.reshape(seq_count, cache_locations, kv_count, head_size)
    scores = (
        jnp.einsum(
            "skgd,spkd->skgp", grouped, key_split, preferred_element_type=jnp.float32
        ).reshape(seq_count, head_count, cache_locations)
        * factor
    )
    positions = jnp.arange(cache_locations, dtype=jnp.int32)
    latest = jnp.sum(
        jnp.where(positions[None, None, :] == (length - 1)[:, None, None], cumulative, 0.0), axis=-1
    )
    scores = scores + (latest + log_gate)[..., None] - cumulative
    valid = positions[None, None, :] < length[:, None, None]
    scores = jnp.where(valid, scores, -jnp.inf)
    own_score = (
        jnp.einsum("skgd,skd->skg", grouped, key_new, preferred_element_type=jnp.float32).reshape(
            seq_count, head_count
        )
        * factor
    )
    highest = jnp.maximum(jnp.max(scores, axis=-1), own_score)
    raised = jnp.exp(scores - highest[..., None])
    own_raised = jnp.exp(own_score - highest)
    denominator = jnp.sum(raised, axis=-1) + own_raised
    weights = (raised / denominator[..., None]).astype(jnp.bfloat16)
    own_weight = (own_raised / denominator).astype(jnp.bfloat16)
    mixed = jnp.einsum(
        "skgp,spkd->skgd",
        weights.reshape(seq_count, kv_count, group_size, cache_locations),
        value_split,
        preferred_element_type=jnp.float32,
    )
    mixed = (
        mixed
        + own_weight.reshape(seq_count, kv_count, group_size)[..., None].astype(jnp.float32)
        * value_new.astype(jnp.float32)[:, :, None, :]
    )
    return mixed.reshape(seq_count, head_count * head_size).astype(jnp.bfloat16)


def expert_work(rows_in, expert_gate, expert_up, expert_down):
    leading = rows_in.shape[:-1]
    flat_rows = rows_in.reshape(-1, rows_in.shape[-1])
    gate_out = jnp.dot(flat_rows, expert_gate, preferred_element_type=jnp.float32)
    up_out = jnp.dot(flat_rows, expert_up, preferred_element_type=jnp.float32)
    hidden = (jax.nn.silu(gate_out) * up_out).astype(jnp.bfloat16)
    return jnp.dot(hidden, expert_down, preferred_element_type=jnp.float32).reshape(
        leading + (expert_down.shape[1],)
    )


def combine(returned, target, route_weights):
    capacity = returned.shape[1]
    columns = returned.shape[2]
    blocks = jnp.sum(
        returned.reshape(EXPERTS, -1, capacity, columns).astype(jnp.float32), axis=1
    ).reshape(EXPERTS * capacity, columns)
    picked = jnp.take(blocks, target, axis=0).reshape(route_weights.shape + (columns,))
    return jnp.sum(picked * route_weights[..., None], axis=1)


def on_device(
    tokens,
    lengths,
    key_cache,
    value_cache,
    gate_cache,
    mix_gain,
    query_weight,
    key_weight,
    value_weight,
    forget_weight,
    out_weight,
    expert_gain,
    routes,
    route_weights,
    expert_gate,
    expert_up,
    expert_down,
):
    seq_count = tokens.shape[0]
    width = tokens.shape[1]
    normal_in = normed(tokens, mix_gain).astype(jnp.bfloat16)
    queries = (
        jnp.dot(normal_in, query_weight, preferred_element_type=jnp.float32)
        .astype(jnp.bfloat16)
        .reshape(seq_count, -1, HD)
    )
    key_new = (
        jnp.dot(normal_in, key_weight, preferred_element_type=jnp.float32)
        .astype(jnp.bfloat16)
        .reshape(seq_count, -1, HD)
    )
    value_new = (
        jnp.dot(normal_in, value_weight, preferred_element_type=jnp.float32)
        .astype(jnp.bfloat16)
        .reshape(seq_count, -1, HD)
    )
    log_gate = jax.nn.log_sigmoid(
        jnp.dot(normal_in, forget_weight, preferred_element_type=jnp.float32)
    )
    mixed = attend(
        queries, key_new, value_new, log_gate, key_cache, value_cache, gate_cache, lengths
    )
    partial_out = jnp.dot(mixed, out_weight, preferred_element_type=jnp.float32).astype(
        jnp.bfloat16
    )
    residual = (
        tokens.astype(jnp.float32) + lax.psum(partial_out, "tp").astype(jnp.float32)
    ).astype(jnp.bfloat16)
    expert_in = normed(residual, expert_gain).astype(jnp.bfloat16)
    top_count = routes.shape[1]
    flat_routes = routes.reshape(-1)
    one_hot = (flat_routes[:, None] == jnp.arange(EXPERTS, dtype=jnp.int32)[None, :]).astype(
        jnp.int32
    )
    slot_index = jnp.sum((jnp.cumsum(one_hot, axis=0) - 1) * one_hot, axis=1)
    target = flat_routes * CAP + slot_index
    dispatch = (jnp.arange(EXPERTS * CAP, dtype=jnp.int32)[:, None] == target[None, :]).astype(
        jnp.bfloat16
    )
    repeated = jnp.repeat(expert_in, top_count, axis=0)
    outgoing = jnp.dot(dispatch, repeated, preferred_element_type=jnp.float32).astype(jnp.bfloat16)
    pieces = lax.axis_size("ep") // EXPERTS
    outgoing = jnp.broadcast_to(
        outgoing.reshape(EXPERTS, 1, CAP, width), (EXPERTS, pieces, CAP, width)
    ).reshape(EXPERTS * pieces, CAP, width)
    half_width = width // lax.axis_size("tp")
    start = lax.axis_index("tp") * half_width
    outgoing_half = lax.dynamic_slice_in_dim(outgoing, start, half_width, 2)
    full_rows = lax.all_gather(
        lax.all_to_all(outgoing_half, "ep", split_axis=0, concat_axis=0, tiled=True),
        "tp",
        axis=2,
        tiled=True,
    )
    partial_rows = expert_work(full_rows, expert_gate, expert_up, expert_down).astype(jnp.bfloat16)
    share = (
        lax.psum_scatter(partial_rows, "tp", scatter_dimension=2, tiled=True)
        .astype(jnp.float32)
        .astype(jnp.bfloat16)
    )
    returned = lax.all_to_all(share, "ep", split_axis=0, concat_axis=0, tiled=True)
    mixture = combine(returned, target, route_weights)
    own_half = lax.dynamic_slice_in_dim(residual, start, half_width, 1).astype(jnp.float32)
    return lax.all_gather((own_half + mixture).astype(jnp.bfloat16), "tp", axis=1, tiled=True)


def solution(mesh):
    return jax.shard_map(
        on_device,
        mesh=mesh,
        in_specs=(
            P("ep", None),
            P("ep"),
            P("ep", None, "tp"),
            P("ep", None, "tp"),
            P("ep", "tp", None),
            P(),
            P(None, "tp"),
            P(None, "tp"),
            P(None, "tp"),
            P(None, "tp"),
            P("tp", None),
            P(),
            P("ep", None),
            P("ep", None),
            P(None, ("ep", "tp")),
            P(None, ("ep", "tp")),
            P(("ep", "tp"), None),
        ),
        out_specs=P("ep", None),
        check_vma=False,
    )
```

profile of v0, /device:TPU:0, one launch (start us, length us, event | category | flops | bytes accessed | tf_op | source)
XLA Modules:
  0.0 167.7 jit_solution(255999665573253015)
XLA Ops:
  6.5 0.8 broadcast_add_fusion
  7.3 0.7 iota_compare_fusion.1
  8.1 1.0 fusion.7
  9.1 2.2 %convolution_convert_fusion.3 = bf16[32,512]{1,0:T(8,128)(2,1)S(1)} fusion(bf16[2048,512]{1,0:T(8,128)(2,1)} %param.23, bf16[32,2048]{1,0:T(8,128)(2,1)} %param.17, f32[2048]{0:T(1024)} %param.22, f32[32]{0:T(128)S(1)} %add_rsqrt_fusion.1), kind=kOutput, calls=%fused_computation.9 | convolution fusion | flops 67387392 | bytes 2269312 | tf_op jit(solution)/shard_map/dot_general | solution.py:109
  11.3 0.1 reshape_reshape.3
  11.5 11.9 %copy.45 = bf16[32,1024,128]{1,2,0:T(8,128)(2,1)} copy(bf16[32,1024,128]{2,1,0:T(8,128)(2,1)} %param.19) | data formatting | bytes 16777216 | tf_op args[2]
  23.4 4.6 %convolution_multiply_fusion.1 = f32[32,2,4,1024]{3,2,1,0:T(4,128)S(1)} fusion(bf16[32,2,4,64]{3,2,1,0:T(4,128)(2,1)S(1)} %reshape_reshape.3, bf16[32,1024,2,64]{1,3,2,0:T(8,128)(2,1)} %bitcast.37), kind=kOutput, calls=%fused_computation.6 | convolution fusion | flops 33816576 | bytes 9469952 | tf_op jit(solution)/shard_map/skgd,spkd->skgp/dot_general | solution.py:27
  28.0 1.4 mul.132
  29.4 0.1 iota_compare_fusion
  29.5 1.5 select_reduce_fusion
  31.0 0.2 fusion.15
  31.2 0.1 copy.47
  31.3 1.9 %fusion.25 = (f32[32,8]{1,0:T(8,128)S(1)}, f32[32,8,1024]{2,1,0:T(8,128)S(1)}) fusion(f32[32,8,1024]{2,1,0:T(8,128)} %param.21, f32[32,8,1024]{2,1,0:T(8,128)} %mul.132, f32[32,8]{1,0:T(8,128)S(1)} %copy.47, pred[32,1024]{1,0:T(8,128)(4,1)S(1)} %iota_compare_fusion.1), kind=kLoop, calls=%fused_computation.64 | loop fusion | flops 1048320 | bytes 3180544 | tf_op jit(solution)/shard_map/reduce_max | solution.py:45
  33.3 1.3 convolution_convert_fusion.5
  34.6 0.1 reshape.208
  34.7 0.2 fusion.26
  34.9 0.1 copy.62
  35.0 0.1 copy.49
  35.1 0.3 fusion.3
  35.5 0.1 copy.51
  35.5 1.1 divide_convert_fusion
  36.6 1.2 reshape.188
  37.9 0.1 copy.55
  38.0 1.3 fusion.2
  39.3 0.1 reshape.195
  39.4 11.9 %copy.52 = bf16[32,1024,128]{1,2,0:T(8,128)(2,1)} copy(bf16[32,1024,128]{2,1,0:T(8,128)(2,1)} %param.20) | data formatting | bytes 16777216 | tf_op args[3]
  51.3 5.7 %fusion.1 = bf16[32,2,4,64]{3,2,1,0:T(4,128)(2,1)S(1)} fusion(bf16[32,2,4,1024]{3,2,1,0:T(4,128)(2,1)S(1)} %reshape.188, bf16[32,1024,2,64]{1,3,2,0:T(8,128)(2,1)} %bitcast.38, f32[32,2,64]{2,1,0:T(2,128)S(1)} %reshape.195, f32[32,2,4]{2,1,0:T(2,128)S(1)} %copy.55), kind=kOutput, calls=%fused_computation.8 | convolution fusion | flops 33603584 | bytes 8963072 | tf_op jit(solution)/shard_map/skgp,spkd->skgd/dot_general | solution.py:51
  57.0 0.1 convert_element_type.99
  57.1 1.1 convolution_convert_fusion.2
  58.4 0.1 copy.56
  58.5 0.1 reshape.190
  58.6 0.1 reduce_window_sum.11
  58.7 0.2 select_reduce_fusion.1
  58.9 20.2 %all-reduce.2.cloned.1.call-done = bf16[32,2048]{1,0:T(8,128)(2,1)} async-done(((bf16[32,2048]{1,0:T(8,128)(2,1)}), bf16[32,2048]{1,0:T(8,128)(2,1)}) %all-reduce.2.cloned.1.call-update) | async-done | bytes 131088 | tf_op jit(solution)/shard_map/psum | solution.py:133
  79.1 1.1 fusion.4
  80.2 0.1 fusion.6
  80.3 0.5 copy-done.3
  80.8 0.1 broadcast_in_dim.61
  81.0 0.1 reshape.191
  81.1 0.2 convolution_convert_fusion.1
  81.3 0.1 broadcast_in_dim.62
  81.4 0.1 broadcast_in_dim.63
  81.6 22.1 %all_to_all.10 = bf16[16,12,1024]{2,1,0:T(8,128)(2,1)S(1)} all-to-all(bf16[16,12,1024]{2,1,0:T(8,128)(2,1)S(1)} %constant_dynamic-slice_fusion), channel_id=1, replica_groups=mesh['ep'=16,'tp'=2] {'ep'}, dimensions={0} | all-to-all | bytes 786432 | tf_op jit(solution)/shard_map/all_to_all | solution.py:156
  103.7 2.7 %all_gather.6 = bf16[16,12,2048]{2,1,0:T(8,128)(2,1)S(1)} all-gather(bf16[16,12,1024]{2,1,0:T(8,128)(2,1)S(1)} %all_to_all.10), channel_id=1, replica_groups=mesh['ep'=16,'tp'=2] {'tp'}, dimensions={2}, use_global_device_ids=true | all-gather | bytes 1179648 | tf_op jit(solution)/shard_map/all_gather | solution.py:155
  106.5 0.2 reshape.193
  106.6 6.3 %fusion.27 = f32[192,2048]{1,0:T(8,128)} fusion(bf16[192,2048]{1,0:T(8,128)(2,1)S(1)} %reshape.193, bf16[2048,2048]{1,0:T(8,128)(2,1)} %param.31), kind=kOutput, calls=%fused_computation.66 | convolution fusion | flops 1610612736 | bytes 10747904 | tf_op jit(solution)/shard_map/dot_general | solution.py:68
  113.0 10.9 %convolution_convert_fusion = bf16[192,2048]{1,0:T(8,128)(2,1)} fusion(bf16[2048,2048]{1,0:T(8,128)(2,1)} %param.33, bf16[192,2048]{1,0:T(8,128)(2,1)S(1)} %reshape.193, bf16[2048,2048]{1,0:T(8,128)(2,1)} %param.32, f32[192,2048]{1,0:T(8,128)} %fusion.27), kind=kOutput, calls=%fused_computation.2 | convolution fusion | flops 3223977984 | bytes 19922944 | tf_op jit(solution)/shard_map/dot_general | solution.py:71
  123.8 2.1 %convert_element_type.110 = bf16[16,12,2048]{2,1,0:T(8,128)(2,1)} reshape(bf16[192,2048]{1,0:T(8,128)(2,1)} %convolution_convert_fusion) | data formatting | bytes 1572864 | tf_op jit(solution)/shard_map/convert_element_type | solution.py:161
  126.0 0.1 reduce_sum.74
  126.1 6.8 %reduce-scatter.2.cloned.1.call-done = bf16[16,12,1024]{2,1,0:T(8,128)(2,1)} async-done(((bf16[16,12,2048]{2,1,0:T(8,128)(2,1)}), bf16[16,12,1024]{2,1,0:T(8,128)(2,1)}) %reduce-scatter.2.cloned.1.call-update) | async-done | bytes 393232 | tf_op jit(solution)/shard_map/reduce_scatter | solution.py:163
  132.9 6.8 %all-to-all-start.1 = ((bf16[16,12,1024]{2,1,0:T(8,128)(2,1)}), bf16[16,12,1024]{2,1,0:T(8,128)(2,1)S(1)}, u32[]{:S(2)}, u32[]{:S(2)}) async-start(bf16[16,12,1024]{2,1,0:T(8,128)(2,1)} %reduce-scatter.2.cloned.1.call-done), calls=%async_computation.2 | async-start | bytes 1048576 | tf_op jit(solution)/shard_map/all_to_all | solution.py:167
  139.7 0.1 copy.59
  139.8 0.1 mul.152
  140.0 0.7 copy.58
  140.7 0.1 copy.60
  140.7 0.6 pad_clamp_fusion
  141.3 13.8 %all-to-all-done.1 = bf16[16,12,1024]{2,1,0:T(8,128)(2,1)S(1)} async-done(((bf16[16,12,1024]{2,1,0:T(8,128)(2,1)}), bf16[16,12,1024]{2,1,0:T(8,128)(2,1)S(1)}, u32[]{:S(2)}, u32[]{:S(2)}) %all-to-all-start.1) | async-done | bytes 393248 | tf_op jit(solution)/shard_map/all_to_all | solution.py:167
  155.1 0.1 convert_reduce_fusion
  155.3 0.8 gather_fusion
  156.1 0.1 gather.7
  156.3 1.2 multiply_reduce_fusion
  157.4 0.9 add_convert_fusion
  158.3 1.9 %all_gather.7 = bf16[32,2048]{1,0:T(8,128)(2,1)S(1)} all-gather(bf16[32,1024]{1,0:T(8,128)(2,1)S(1)} %add_convert_fusion), channel_id=1, replica_groups=mesh['ep'=16,'tp'=2] {'tp'}, dimensions={1}, use_global_device_ids=true | all-gather | bytes 196608 | tf_op jit(solution)/shard_map/all_gather | solution.py:170
  160.2 0.7 copy.65
  (38 shorter events, 0.6 us)
Async XLA Ops:
  6.5 50.6 %copy-start = (bf16[512,2048]{1,0:T(8,128)(2,1)S(1)}, bf16[512,2048]{1,0:T(8,128)(2,1)}, u32[]{:S(2)}) copy-start(bf16[512,2048]{1,0:T(8,128)(2,1)} %param.27) | copy-start | bytes 6291460
  6.5 72.6 %all-reduce.2.cloned.1.call-start = ((), (), s32[]{:S(2)}) async-start(), calls=%async_computation.3 | async-start | bytes 262144 | tf_op jit(solution)/shard_map/psum | solution.py:133
  23.4 7.6 %copy-start.2 = (bf16[32,2048]{1,0:T(8,128)(2,1)S(1)}, bf16[32,2048]{1,0:T(8,128)(2,1)}, u32[]{:S(2)}) copy-start(bf16[32,2048]{1,0:T(8,128)(2,1)} %param.17) | copy-start | bytes 393220
  23.4 7.6 %copy-start.4 = (f32[2048]{0:T(1024)S(1)}, f32[2048]{0:T(1024)}, u32[]{:S(2)}) copy-start(f32[2048]{0:T(1024)} %param.22) | copy-start | bytes 24580
  23.4 7.6 %copy-start.8 = (bf16[2048,8]{0,1:T(8,128)(2,1)S(1)}, bf16[2048,8]{0,1:T(8,128)(2,1)}, u32[]{:S(2)}) copy-start(bf16[2048,8]{0,1:T(8,128)(2,1)} %param.26) | copy-start | bytes 98308
  51.3 7.0 %copy-start.5 = (s32[32,2]{0,1:T(2,128)S(1)}, s32[32,2]{0,1:T(2,128)}, u32[]{:S(2)}) copy-start(s32[32,2]{0,1:T(2,128)} %param.29) | copy-start | bytes 772
  51.3 28.9 %copy-start.6 = (f32[2048]{0:T(1024)S(1)}, f32[2048]{0:T(1024)}, u32[]{:S(2)}) copy-start(f32[2048]{0:T(1024)} %param.28) | copy-start | bytes 24580
  58.3 74.6 %reduce-scatter.2.cloned.1.call-start = ((), (), s32[]{:S(2)}) async-start(), calls=%async_computation.4 | async-start | bytes 1572864 | tf_op jit(solution)/shard_map/reduce_scatter | solution.py:163
  80.2 0.7 copy-start.3
  113.0 27.7 %copy-start.7 = (f32[32,2]{0,1:T(2,128)S(1)}, f32[32,2]{0,1:T(2,128)}, u32[]{:S(2)}) copy-start(f32[32,2]{0,1:T(2,128)} %param.30) | copy-start | bytes 772
  113.0 47.9 %copy-start.1 = (bf16[512,2048]{1,0:T(8,128)(2,1)S(1)}, bf16[512,2048]{1,0:T(8,128)(2,1)}, u32[]{:S(2)}) copy-start(bf16[512,2048]{1,0:T(8,128)(2,1)} %param.27) | copy-start | bytes 6291460
  132.9 22.3 %all-to-all-start.1 = ((bf16[16,12,1024]{2,1,0:T(8,128)(2,1)}), bf16[16,12,1024]{2,1,0:T(8,128)(2,1)S(1)}, u32[]{:S(2)}, u32[]{:S(2)}) async-start(bf16[16,12,1024]{2,1,0:T(8,128)(2,1)} %reduce-scatter.2.cloned.1.call-done), calls=%async_computation.2 | async-start | bytes 1048576 | tf_op jit(solution)/shard_map/all_to_all | solution.py:167
Sparse Core Ops, SparseCore 0:
  58.4 20.6 all-reduce.1
  126.1 6.7 reduce-scatter.1
where the time goes:
time: 169 us; the launch traced here: 168 us
  waiting for transfers between devices  40.8 us (24%)
  matrix products  34.1 us (20%)
  local copies, waits for them, and re-layouts  33.9 us (20%)
  blocking collectives  26.7 us (16%)
  between operations  13.7 us (8%)
  other arithmetic  11.7 us (7%)
  starting transfers between devices  6.82 us (4%)
    unnamed x23, local copies, waits for them, and re-layouts  25.3 us
    all_to_all x1, blocking collectives, on_device(): lax.all_to_all(outgoing_half, 'ep', split_axis=0, concat_axis=0, tiled=True)  22.1 us
    psum x1, waiting for transfers between devices, on_device(): lax.psum(partial_out, 'tp').astype(jnp.float32)  20.2 us
    all_to_all x1, waiting for transfers between devices, on_device(): lax.all_to_all(share, 'ep', split_axis=0, concat_axis=0, tiled=True)  13.8 us
    dot_general x1, matrix products, expert_work(): jnp.dot(hidden, expert_down, preferred_element_type=jnp.float32)  10.9 us
    all_to_all x1, starting transfers between devices, on_device(): lax.all_to_all(share, 'ep', split_axis=0, concat_axis=0, tiled=True)  6.78 us
    reduce_scatter x1, waiting for transfers between devices, on_device(): lax.psum_scatter(partial_rows, 'tp', scatter_dimension=2, tiled=True)  6.77 us
    dot_general x1, matrix products, expert_work(): jnp.dot(flat_rows, expert_gate, preferred_element_type=jnp.float32)  6.34 us
  transfers between devices with their start and end apart: 3, of which 3 were waited for; matrix products, arithmetic and copies ran while one was open for 1% of the time, Pallas kernels for 0%

commit v1 on v0

--- a/solution.py
+++ b/solution.py
@@ -130,7 +130,8 @@
         jnp.bfloat16
     )
     residual = (
-        tokens.astype(jnp.float32) + lax.psum(partial_out, "tp").astype(jnp.float32)
+        tokens.astype(jnp.float32)
+        + jnp.sum(lax.all_gather(partial_out, "tp"), axis=0).astype(jnp.float32)
     ).astype(jnp.bfloat16)
     expert_in = normed(residual, expert_gain).astype(jnp.bfloat16)
     top_count = routes.shape[1]

time: 169 us -> 151 us (0.89)
  waiting for transfers between devices: 40.8 us -> 20.6 us
  blocking collectives: 26.7 us -> 30.1 us
    psum x1 -> x0, waiting for transfers between devices: 20.2 us -> none  [on_device(): lax.psum(partial_out, 'tp').astype(jnp.float32)]
    all_gather x0 -> x1, blocking collectives: none -> 2.12 us  [on_device(): lax.all_gather(partial_out, 'tp')]
  transfers between devices with their start and end apart: 3 -> 2, of which waited for: 3 -> 2; matrix products, arithmetic and copies ran while one was open for 1% -> 1% of each run, Pallas kernels for 0% -> 0%
where the time goes in v1:
time: 151 us; the launch traced here: 149 us
  local copies, waits for them, and re-layouts  33.9 us (22%)
  matrix products  33.4 us (22%)
  blocking collectives  30.1 us (20%)
  waiting for transfers between devices  20.6 us (14%)
  between operations  13.6 us (9%)
  other arithmetic  10.9 us (7%)
  starting transfers between devices  6.78 us (4%)
    unnamed x23, local copies, waits for them, and re-layouts  25.3 us
    all_to_all x1, blocking collectives, on_device(): lax.all_to_all(outgoing_half, 'ep', split_axis=0, concat_axis=0, tiled=True)  23.4 us
    all_to_all x1, waiting for transfers between devices, on_device(): lax.all_to_all(share, 'ep', split_axis=0, concat_axis=0, tiled=True)  13.8 us
    dot_general x1, matrix products, expert_work(): jnp.dot(hidden, expert_down, preferred_element_type=jnp.float32)  10.9 us
    all_to_all x1, starting transfers between devices, on_device(): lax.all_to_all(share, 'ep', split_axis=0, concat_axis=0, tiled=True)  6.78 us
    reduce_scatter x1, waiting for transfers between devices, on_device(): lax.psum_scatter(partial_rows, 'tp', scatter_dimension=2, tiled=True)  6.77 us
    dot_general x1, matrix products, expert_work(): jnp.dot(flat_rows, expert_gate, preferred_element_type=jnp.float32)  6.34 us
    dot_general x1, matrix products, attend(): jnp.einsum('skgp,spkd->skgd', weights.reshape(seq_count, kv_count, group_...  5.68 us
  transfers between devices with their start and end apart: 2, of which 2 were waited for; matrix products, arithmetic and copies ran while one was open for 1% of the time, Pallas kernels for 0%

profile of v1, /device:TPU:0, one launch (start us, length us, event | category | flops | bytes accessed | tf_op | source)
XLA Modules:
  0.0 149.4 jit_solution(16886828701489950291)
XLA Ops:
  6.5 0.8 broadcast_add_fusion
  7.3 0.7 iota_compare_fusion.1
  8.1 1.0 fusion.7
  9.1 2.2 %convolution_convert_fusion.3 = bf16[32,512]{1,0:T(8,128)(2,1)S(1)} fusion(bf16[2048,512]{1,0:T(8,128)(2,1)} %param.23, bf16[32,2048]{1,0:T(8,128)(2,1)} %param.17, f32[2048]{0:T(1024)} %param.22, f32[32]{0:T(128)S(1)} %add_rsqrt_fusion.1), kind=kOutput, calls=%fused_computation.9 | convolution fusion | flops 67387392 | bytes 2269312 | tf_op jit(solution)/shard_map/dot_general | solution.py:109
  11.3 0.1 reshape_reshape.3
  11.5 11.9 %copy.45 = bf16[32,1024,128]{1,2,0:T(8,128)(2,1)} copy(bf16[32,1024,128]{2,1,0:T(8,128)(2,1)} %param.19) | data formatting | bytes 16777216 | tf_op args[2]
  23.4 4.6 %convolution_multiply_fusion.1 = f32[32,2,4,1024]{3,2,1,0:T(4,128)S(1)} fusion(bf16[32,2,4,64]{3,2,1,0:T(4,128)(2,1)S(1)} %reshape_reshape.3, bf16[32,1024,2,64]{1,3,2,0:T(8,128)(2,1)} %bitcast.38), kind=kOutput, calls=%fused_computation.6 | convolution fusion | flops 33816576 | bytes 9469952 | tf_op jit(solution)/shard_map/skgd,spkd->skgp/dot_general | solution.py:27
  28.0 1.4 mul.132
  29.4 0.1 iota_compare_fusion
  29.5 1.5 select_reduce_fusion
  31.0 0.2 fusion.15
  31.2 0.1 copy.47
  31.3 1.9 %fusion.25 = (f32[32,8]{1,0:T(8,128)S(1)}, f32[32,8,1024]{2,1,0:T(8,128)S(1)}) fusion(f32[32,8,1024]{2,1,0:T(8,128)} %param.21, f32[32,8,1024]{2,1,0:T(8,128)} %mul.132, f32[32,8]{1,0:T(8,128)S(1)} %copy.47, pred[32,1024]{1,0:T(8,128)(4,1)S(1)} %iota_compare_fusion.1), kind=kLoop, calls=%fused_computation.64 | loop fusion | flops 1048320 | bytes 3180544 | tf_op jit(solution)/shard_map/reduce_max | solution.py:45
  33.3 1.3 convolution_convert_fusion.5
  34.6 0.1 reshape.209
  34.7 0.2 fusion.26
  34.9 0.1 copy.62
  35.0 0.1 copy.49
  35.1 0.3 fusion.3
  35.5 0.1 copy.51
  35.6 1.1 divide_convert_fusion
  36.6 1.2 reshape.188
  37.9 0.1 copy.55
  38.0 1.3 fusion.2
  39.3 0.1 reshape.195
  39.4 11.9 %copy.52 = bf16[32,1024,128]{1,2,0:T(8,128)(2,1)} copy(bf16[32,1024,128]{2,1,0:T(8,128)(2,1)} %param.20) | data formatting | bytes 16777216 | tf_op args[3]
  51.3 5.7 %fusion.1 = bf16[32,2,4,64]{3,2,1,0:T(4,128)(2,1)S(1)} fusion(bf16[32,2,4,1024]{3,2,1,0:T(4,128)(2,1)S(1)} %reshape.188, bf16[32,1024,2,64]{1,3,2,0:T(8,128)(2,1)} %bitcast.39, f32[32,2,64]{2,1,0:T(2,128)S(1)} %reshape.195, f32[32,2,4]{2,1,0:T(2,128)S(1)} %copy.55), kind=kOutput, calls=%fused_computation.8 | convolution fusion | flops 33603584 | bytes 8963072 | tf_op jit(solution)/shard_map/skgp,spkd->skgd/dot_general | solution.py:51
  57.0 0.1 convert_element_type.101
  57.2 0.5 convolution_convert_fusion.2
  57.6 2.1 %all-gather = bf16[64,2048]{1,0:T(8,128)(2,1)S(1)} all-gather(bf16[32,2048]{1,0:T(8,128)(2,1)S(1)} %convolution_convert_fusion.2), channel_id=2, replica_groups=mesh['ep'=16,'tp'=2] {'tp'}, dimensions={0}, use_global_device_ids=true | all-gather | bytes 393216 | tf_op jit(solution)/shard_map/all_gather | solution.py:134
  59.8 0.2 fusion.4
  60.0 0.1 fusion.6
  60.1 0.5 copy-done.3
  60.6 0.1 broadcast_in_dim.61
  60.8 0.1 reshape.191
  60.9 0.1 copy.56
  61.0 0.1 reshape.190
  61.1 0.1 reduce_window_sum.11
  61.2 0.2 select_reduce_fusion.1
  61.4 0.2 convolution_convert_fusion.1
  61.7 0.1 broadcast_in_dim.62
  61.8 0.1 broadcast_in_dim.63
  62.0 23.4 %all_to_all.10 = bf16[16,12,1024]{2,1,0:T(8,128)(2,1)S(1)} all-to-all(bf16[16,12,1024]{2,1,0:T(8,128)(2,1)S(1)} %constant_dynamic-slice_fusion), channel_id=1, replica_groups=mesh['ep'=16,'tp'=2] {'ep'}, dimensions={0} | all-to-all | bytes 786432 | tf_op jit(solution)/shard_map/all_to_all | solution.py:157
  85.4 2.7 %all_gather.14 = bf16[16,12,2048]{2,1,0:T(8,128)(2,1)S(1)} all-gather(bf16[16,12,1024]{2,1,0:T(8,128)(2,1)S(1)} %all_to_all.10), channel_id=1, replica_groups=mesh['ep'=16,'tp'=2] {'tp'}, dimensions={2}, use_global_device_ids=true | all-gather | bytes 1179648 | tf_op jit(solution)/shard_map/all_gather | solution.py:156
  88.1 0.2 reshape.193
  88.3 6.3 %fusion.27 = f32[192,2048]{1,0:T(8,128)} fusion(bf16[192,2048]{1,0:T(8,128)(2,1)S(1)} %reshape.193, bf16[2048,2048]{1,0:T(8,128)(2,1)} %param.31), kind=kOutput, calls=%fused_computation.66 | convolution fusion | flops 1610612736 | bytes 10747904 | tf_op jit(solution)/shard_map/dot_general | solution.py:68
  94.6 10.9 %convolution_convert_fusion = bf16[192,2048]{1,0:T(8,128)(2,1)} fusion(bf16[2048,2048]{1,0:T(8,128)(2,1)} %param.33, bf16[192,2048]{1,0:T(8,128)(2,1)S(1)} %reshape.193, bf16[2048,2048]{1,0:T(8,128)(2,1)} %param.32, f32[192,2048]{1,0:T(8,128)} %fusion.27), kind=kOutput, calls=%fused_computation.2 | convolution fusion | flops 3223977984 | bytes 19922944 | tf_op jit(solution)/shard_map/dot_general | solution.py:71
  105.5 2.1 %convert_element_type.112 = bf16[16,12,2048]{2,1,0:T(8,128)(2,1)} reshape(bf16[192,2048]{1,0:T(8,128)(2,1)} %convolution_convert_fusion) | data formatting | bytes 1572864 | tf_op jit(solution)/shard_map/convert_element_type | solution.py:162
  107.6 0.1 reduce_sum.87
  107.7 6.8 %reduce-scatter.2.cloned.1.call-done = bf16[16,12,1024]{2,1,0:T(8,128)(2,1)} async-done(((bf16[16,12,2048]{2,1,0:T(8,128)(2,1)}), bf16[16,12,1024]{2,1,0:T(8,128)(2,1)}) %reduce-scatter.2.cloned.1.call-update) | async-done | bytes 393232 | tf_op jit(solution)/shard_map/reduce_scatter | solution.py:164
  114.5 6.8 %all-to-all-start.1 = ((bf16[16,12,1024]{2,1,0:T(8,128)(2,1)}), bf16[16,12,1024]{2,1,0:T(8,128)(2,1)S(1)}, u32[]{:S(2)}, u32[]{:S(2)}) async-start(bf16[16,12,1024]{2,1,0:T(8,128)(2,1)} %reduce-scatter.2.cloned.1.call-done), calls=%async_computation.2 | async-start | bytes 1048576 | tf_op jit(solution)/shard_map/all_to_all | solution.py:168
  121.3 0.1 copy.59
  121.4 0.1 mul.152
  121.6 0.7 copy.58
  122.3 0.1 copy.60
  122.4 0.6 pad_clamp_fusion
  123.0 13.8 %all-to-all-done.1 = bf16[16,12,1024]{2,1,0:T(8,128)(2,1)S(1)} async-done(((bf16[16,12,1024]{2,1,0:T(8,128)(2,1)}), bf16[16,12,1024]{2,1,0:T(8,128)(2,1)S(1)}, u32[]{:S(2)}, u32[]{:S(2)}) %all-to-all-start.1) | async-done | bytes 393248 | tf_op jit(solution)/shard_map/all_to_all | solution.py:168
  136.8 0.1 convert_reduce_fusion
  136.9 0.8 gather_fusion
  137.8 0.1 gather.7
  137.9 1.2 multiply_reduce_fusion
  139.1 0.9 add_convert_fusion
  139.9 1.9 %all_gather.15 = bf16[32,2048]{1,0:T(8,128)(2,1)S(1)} all-gather(bf16[32,1024]{1,0:T(8,128)(2,1)S(1)} %add_convert_fusion), channel_id=1, replica_groups=mesh['ep'=16,'tp'=2] {'tp'}, dimensions={1}, use_global_device_ids=true | all-gather | bytes 196608 | tf_op jit(solution)/shard_map/all_gather | solution.py:171
  141.8 0.7 copy.64
  (37 shorter events, 0.6 us)
Async XLA Ops:
  6.5 50.6 %copy-start = (bf16[512,2048]{1,0:T(8,128)(2,1)S(1)}, bf16[512,2048]{1,0:T(8,128)(2,1)}, u32[]{:S(2)}) copy-start(bf16[512,2048]{1,0:T(8,128)(2,1)} %param.27) | copy-start | bytes 6291460
  6.5 108.0 %reduce-scatter.2.cloned.1.call-start = ((), (), s32[]{:S(2)}) async-start(), calls=%async_computation.3 | async-start | bytes 1572864 | tf_op jit(solution)/shard_map/reduce_scatter | solution.py:164
  23.4 7.6 %copy-start.2 = (bf16[32,2048]{1,0:T(8,128)(2,1)S(1)}, bf16[32,2048]{1,0:T(8,128)(2,1)}, u32[]{:S(2)}) copy-start(bf16[32,2048]{1,0:T(8,128)(2,1)} %param.17) | copy-start | bytes 393220
  23.4 7.6 %copy-start.4 = (f32[2048]{0:T(1024)S(1)}, f32[2048]{0:T(1024)}, u32[]{:S(2)}) copy-start(f32[2048]{0:T(1024)} %param.22) | copy-start | bytes 24580
  23.4 7.6 %copy-start.8 = (bf16[2048,8]{0,1:T(8,128)(2,1)S(1)}, bf16[2048,8]{0,1:T(8,128)(2,1)}, u32[]{:S(2)}) copy-start(bf16[2048,8]{0,1:T(8,128)(2,1)} %param.26) | copy-start | bytes 98308
  51.3 8.6 %copy-start.6 = (f32[2048]{0:T(1024)S(1)}, f32[2048]{0:T(1024)}, u32[]{:S(2)}) copy-start(f32[2048]{0:T(1024)} %param.28) | copy-start | bytes 24580
  51.3 9.5 %copy-start.5 = (s32[32,2]{0,1:T(2,128)S(1)}, s32[32,2]{0,1:T(2,128)}, u32[]{:S(2)}) copy-start(s32[32,2]{0,1:T(2,128)} %param.29) | copy-start | bytes 772
  59.9 0.7 copy-start.3
  94.6 27.7 %copy-start.7 = (f32[32,2]{0,1:T(2,128)S(1)}, f32[32,2]{0,1:T(2,128)}, u32[]{:S(2)}) copy-start(f32[32,2]{0,1:T(2,128)} %param.30) | copy-start | bytes 772
  94.6 47.9 %copy-start.1 = (bf16[512,2048]{1,0:T(8,128)(2,1)S(1)}, bf16[512,2048]{1,0:T(8,128)(2,1)}, u32[]{:S(2)}) copy-start(bf16[512,2048]{1,0:T(8,128)(2,1)} %param.27) | copy-start | bytes 6291460
  114.5 22.3 %all-to-all-start.1 = ((bf16[16,12,1024]{2,1,0:T(8,128)(2,1)}), bf16[16,12,1024]{2,1,0:T(8,128)(2,1)S(1)}, u32[]{:S(2)}, u32[]{:S(2)}) async-start(bf16[16,12,1024]{2,1,0:T(8,128)(2,1)} %reduce-scatter.2.cloned.1.call-done), calls=%async_computation.2 | async-start | bytes 1048576 | tf_op jit(solution)/shard_map/all_to_all | solution.py:168
Sparse Core Ops, SparseCore 0:
  107.8 6.7 reduce-scatter.1
